TPU v7x, 32 devices: a whole 2x2x4 slice. The times are simulated.
32 devices in a mesh: sp: 16 (over z, y, core), tp: 2 (over x).
Axes of the slice: x: 2, y: 2, z: 4, core: 2. Of those that a mesh axis runs over, the one named last changes fastest.
Arguments:
- tokens_in: bfloat16 [4096, 2048], P('sp', 'tp'), may hold values from -400 to 400
- norm_gain: float32 [2048], replicated, may hold values from 0.1 to 1.9
- w_query: bfloat16 [2048, 1024], P('sp', 'tp'), may hold values from -0.125 to 0.125
- w_forget: bfloat16 [2048, 1024], P('sp', 'tp'), may hold values from -0.125 to 0.125
- w_input: bfloat16 [2048, 1024], P('sp', 'tp'), may hold values from -0.125 to 0.125
- w_rgate: bfloat16 [2048, 1024], P('sp', 'tp'), may hold values from -0.125 to 0.125
- w_pool_in: bfloat16 [2048, 1024], P('sp', 'tp'), may hold values from -0.125 to 0.125
- w_pgate: bfloat16 [2048, 1024], P('sp', 'tp'), may hold values from -0.125 to 0.125
- floor_rate: float32 [1024], P('tp'), as said below
- extra_logdecay: float32 [4096, 8], P('sp', 'tp'), as said below
- state_gain: float32 [1024], P('tp'), may hold values from 0.1 to 1.9
- pool_mix: bfloat16 [8, 128, 128], P('tp'), may hold values from -0.5 to 0.5
- pool_gain: float32 [1024], P('tp'), may hold values from 0.1 to 1.9
- out_rec: bfloat16 [1024, 2048], P('tp', 'sp'), may hold values from -0.125 to 0.125
- out_pool: bfloat16 [1024, 2048], P('tp', 'sp'), may hold values from -0.125 to 0.125
- post_gain: float32 [2048], replicated, may hold values from 0.1 to 1.9
Outputs:
- mixed_out: bfloat16 [4096, 2048], P(('sp', 'tp'))
Inputs may be any that keep to these rules, and one draw needn't show every extreme that they name: `floor_rate`: every entry is positive. `extra_logdecay`: every entry is at most zero.
All inputs are finite; a program needn't handle non-finite values.
Results may differ from a plain program's by a relative error of at most 0.015.
Values may be sent and summed in bfloat16 or wider, within the bound.
A program may use at most 64 MiB of HBM per device.

v0:
```python
import jax
import jax.numpy as jnp
from jax import lax
from jax.sharding import PartitionSpec as P

DK = 128
BLOCK = 64
eps = 1e-06
coarsest_scale_depth = lax.Precision.HIGHEST


def prefix(part, axis, combine, identity):
    place = lax.axis_index(axis)
    gathered = jax.tree.map(lambda a: lax.all_gather(a, axis), part)
    state = jax.tree.map(lambda a, e: jnp.zeros_like(a) + jnp.asarray(e, a.dtype), part, identity)

    def one(turn, state):
        return combine(
            state, jax.tree.map(lambda a: lax.dynamic_index_in_dim(a, turn, 0, False), gathered)
        )

    return lax.fori_loop(0, place, one, state)


def shifted(value, axis, steps):
    count = lax.axis_size(axis)
    initial, last = (max(0, -steps), min(count, count - steps))
    return lax.ppermute(value, axis, [(source, source + steps) for source in range(initial, last)])


def chain_merge(earlier, later):
    return (earlier[0] * later[0], later[0][..., None] * earlier[1] + later[1])


def local_blocks(qs, keys, values, logs):
    causal = jnp.arange(BLOCK)[:, None] >= jnp.arange(BLOCK)[None, :]
    heads_dev = qs.shape[1]

    def advance(carry, member):
        carried_memory_matrix, start = carry
        probe_segment, key_piece, input_piece, gc = member
        prefix_sum_vector = jnp.cumsum(gc, axis=1)
        last_index = prefix_sum_vector[:, -1]
        cross_segment_contribution = jnp.einsum(
            "abz,azy->aby",
            probe_segment * jnp.exp(prefix_sum_vector),
            carried_memory_matrix,
            precision=coarsest_scale_depth,
        )
        diff = prefix_sum_vector[:, :, None, :] - prefix_sum_vector[:, None, :, :]
        weight = jnp.where(causal[None, :, :, None], jnp.exp(jnp.minimum(diff, 0.0)), 0.0)
        scores = jnp.einsum(
            "htk,hsk,htsk->hts", probe_segment, key_piece, weight, precision=coarsest_scale_depth
        )
        final_result = cross_segment_contribution + jnp.einsum(
            "hts,hsv->htv", scores, input_piece, precision=coarsest_scale_depth
        )
        carried_memory_matrix = jnp.exp(last_index)[..., None] * carried_memory_matrix + jnp.einsum(
            "njp,njq->npq",
            key_piece * jnp.exp(last_index[:, None, :] - prefix_sum_vector),
            input_piece,
            precision=coarsest_scale_depth,
        )
        pool_reach = probe_segment * jnp.exp(start[:, None, :] + prefix_sum_vector)
        return ((carried_memory_matrix, start + last_index), (final_result, pool_reach))

    begin = (jnp.zeros((heads_dev, DK, DK), jnp.float32), jnp.zeros((heads_dev, DK), jnp.float32))
    (carried_memory_matrix, total), (final_result, pool_reach) = lax.scan(
        advance, begin, (qs, keys, values, logs)
    )
    return (carried_memory_matrix, total, final_result, pool_reach)


def per_device(
    tokens_in,
    norm_gain,
    w_query,
    w_forget,
    w_input,
    w_rgate,
    w_pool_in,
    w_pgate,
    floor_rate,
    extra_logdecay,
    state_gain,
    pool_mix,
    pool_gain,
    out_rec,
    out_pool,
    post_gain,
):
    gathered = (
        lax.all_gather(w_query, "sp", axis=0, tiled=True),
        lax.all_gather(w_forget, "sp", axis=0, tiled=True),
        lax.all_gather(w_input, "sp", axis=0, tiled=True),
        lax.all_gather(w_rgate, "sp", axis=0, tiled=True),
        lax.all_gather(w_pool_in, "sp", axis=0, tiled=True),
        lax.all_gather(w_pgate, "sp", axis=0, tiled=True),
    )
    joined = jnp.concatenate(gathered, axis=1)
    head_cols = w_query.shape[1]
    positions = tokens_in.shape[0]
    model_width = norm_gain.shape[0]
    wide = lax.all_gather(tokens_in, "tp", axis=1, tiled=True).astype(jnp.float32)
    scaled = (wide * norm_gain[None, :]).astype(jnp.bfloat16)
    totals = jnp.dot(scaled, joined, preferred_element_type=jnp.float32)
    squares = jnp.sum(wide * wide, axis=1)
    inv_rms = lax.rsqrt(squares / model_width + eps)
    proj = (totals * inv_rms[:, None]).astype(jnp.bfloat16)
    query = proj[:, 0:head_cols]
    forget = proj[:, head_cols : 2 * head_cols]
    inputs = proj[:, 2 * head_cols : 3 * head_cols]
    rgate = proj[:, 3 * head_cols : 4 * head_cols]
    pool_in = proj[:, 4 * head_cols : 5 * head_cols]
    pgate = proj[:, 5 * head_cols : 6 * head_cols]
    heads_dev = head_cols // DK
    blocks = positions // BLOCK

    def to_blocks(array):
        return array.reshape(blocks, BLOCK, heads_dev, DK).transpose(0, 2, 1, 3)

    forget32 = forget.astype(jnp.float32)
    key_gate = -jnp.expm1(-floor_rate)[None, :] * jax.nn.sigmoid(-forget32)
    log_forget = jnp.log1p(-key_gate) + jnp.repeat(extra_logdecay, DK, axis=1)
    qs = query.astype(jnp.float32) * DK ** (-0.5)
    carried_memory_matrix, total, final_result, pool_reach = local_blocks(
        to_blocks(qs),
        to_blocks(key_gate),
        to_blocks(inputs.astype(jnp.float32)),
        to_blocks(log_forget),
    )
    decays = jnp.exp(total)
    tail_rows = pool_in[positions - 16 :]
    carried = prefix(
        (decays, carried_memory_matrix),
        "sp",
        chain_merge,
        (jnp.ones_like(decays), jnp.zeros_like(carried_memory_matrix)),
    )
    incoming_state = carried[1]
    previous = shifted(tail_rows, "sp", 1).astype(jnp.float32)
    recurrent_output = final_result + jnp.einsum(
        "izaf,zfu->izau", pool_reach, incoming_state, precision=coarsest_scale_depth
    )
    grouped = recurrent_output.transpose(0, 2, 1, 3).reshape(positions, heads_dev, DK)
    normed = grouped * lax.rsqrt(jnp.mean(grouped * grouped, axis=2, keepdims=True) + eps)
    y_rec = (
        normed.reshape(positions, head_cols)
        * state_gain[None, :]
        * jax.nn.silu(rgate.astype(jnp.float32))
    ).astype(jnp.bfloat16)
    group = lax.axis_index("tp") * heads_dev + jnp.arange(head_cols) // DK
    window = jnp.power(2, 1 + group % 4).astype(jnp.int32)
    pool32 = pool_in.astype(jnp.float32)
    extended = jnp.concatenate([previous, pool32], axis=0)
    summed_rows = jnp.zeros((positions, head_cols), jnp.float32)
    for offset in range(16):
        rows_back = extended[16 - offset : 16 - offset + positions]
        summed_rows = summed_rows + jnp.where((offset < window)[None, :], rows_back, 0.0)
    place = lax.axis_index("sp") * positions + jnp.arange(positions)
    count = jnp.minimum(place[:, None] + 1, window[None, :]).astype(jnp.float32)
    mixed = (summed_rows / count - pool32).astype(jnp.bfloat16)
    mapped = jnp.einsum(
        "tgc,gcd->tgd",
        mixed.reshape(positions, heads_dev, DK),
        pool_mix,
        preferred_element_type=jnp.float32,
    ).reshape(positions, head_cols)
    y_pool = (mapped * pool_gain[None, :] * jax.nn.silu(pgate.astype(jnp.float32))).astype(
        jnp.bfloat16
    )
    out_parts = (
        lax.all_gather(out_rec, "sp", axis=1, tiled=True),
        lax.all_gather(out_pool, "sp", axis=1, tiled=True),
    )
    both = jnp.concatenate([y_rec, y_pool], axis=1)
    weight_cat = jnp.concatenate(out_parts, axis=0)
    summed = lax.psum_scatter(
        jnp.dot(both, weight_cat, preferred_element_type=jnp.float32).astype(jnp.bfloat16),
        "tp",
        scatter_dimension=0,
        tiled=True,
    ).astype(jnp.float32)
    final = (
        summed
        * lax.rsqrt(jnp.mean(summed * summed, axis=1, keepdims=True) + eps)
        * post_gain[None, :]
    )
    return final.astype(jnp.bfloat16)


def solution(mesh):
    placed = (
        P("sp", "tp"),
        P(),
        P("sp", "tp"),
        P("sp", "tp"),
        P("sp", "tp"),
        P("sp", "tp"),
        P("sp", "tp"),
        P("sp", "tp"),
        P("tp"),
        P("sp", "tp"),
        P("tp"),
        P("tp", None, None),
        P("tp"),
        P("tp", "sp"),
        P("tp", "sp"),
        P(),
    )
    return jax.shard_map(
        per_device, mesh=mesh, in_specs=placed, out_specs=P(("sp", "tp"), None), check_vma=False
    )
```

profile of v0, /device:TPU:0, one launch (start us, length us, event | category | flops | bytes accessed | tf_op | source)
XLA Modules:
  0.0 518.1 jit_solution(14276728240443677830)
XLA Ops:
  12.8 20.1 %all-gather.14.cloned.1.call-done = bf16[256,2048]{1,0:T(8,128)(2,1)} async-done(((bf16[256,1024]{1,0:T(8,128)(2,1)}), bf16[256,2048]{1,0:T(8,128)(2,1)}) %all-gather.14.cloned.1.call-update) | async-done | bytes 1048592 | tf_op jit(solution)/shard_map/all_gather | solution.py:104
  34.4 42.1 %all-gather.16.cloned.1.call-done = bf16[2048,512]{1,0:T(8,128)(2,1)} async-done(((bf16[128,512]{1,0:T(8,128)(2,1)}), bf16[2048,512]{1,0:T(8,128)(2,1)}) %all-gather.16.cloned.1.call-update) | async-done | bytes 2097168 | tf_op jit(solution)/shard_map/all_gather | solution.py:93
  76.6 3.2 constant_dynamic-update-slice_fusion.5
  79.7 39.2 %all-gather.18.cloned.1.call-done = bf16[2048,512]{1,0:T(8,128)(2,1)} async-done(((bf16[128,512]{1,0:T(8,128)(2,1)}), bf16[2048,512]{1,0:T(8,128)(2,1)}) %all-gather.18.cloned.1.call-update) | async-done | bytes 2097168 | tf_op jit(solution)/shard_map/all_gather | solution.py:94
  118.9 3.2 constant_dynamic-update-slice_fusion.4
  122.2 39.0 %all-gather.20.cloned.1.call-done = bf16[2048,512]{1,0:T(8,128)(2,1)} async-done(((bf16[128,512]{1,0:T(8,128)(2,1)}), bf16[2048,512]{1,0:T(8,128)(2,1)}) %all-gather.20.cloned.1.call-update) | async-done | bytes 2097168 | tf_op jit(solution)/shard_map/all_gather | solution.py:95
  161.2 3.1 constant_dynamic-update-slice_fusion.3
  164.3 39.1 %all-gather.22.cloned.1.call-done = bf16[2048,512]{1,0:T(8,128)(2,1)} async-done(((bf16[128,512]{1,0:T(8,128)(2,1)}), bf16[2048,512]{1,0:T(8,128)(2,1)}) %all-gather.22.cloned.1.call-update) | async-done | bytes 2097168 | tf_op jit(solution)/shard_map/all_gather | solution.py:96
  203.4 3.2 constant_dynamic-update-slice_fusion.2
  206.6 39.0 %all-gather.24.cloned.1.call-done = bf16[2048,512]{1,0:T(8,128)(2,1)} async-done(((bf16[128,512]{1,0:T(8,128)(2,1)}), bf16[2048,512]{1,0:T(8,128)(2,1)}) %all-gather.24.cloned.1.call-update) | async-done | bytes 2097168 | tf_op jit(solution)/shard_map/all_gather | solution.py:97
  245.6 3.2 constant_dynamic-update-slice_fusion.1
  248.8 39.1 %all-gather.26.cloned.1.call-done = bf16[2048,512]{1,0:T(8,128)(2,1)} async-done(((bf16[128,512]{1,0:T(8,128)(2,1)}), bf16[2048,512]{1,0:T(8,128)(2,1)}) %all-gather.26.cloned.1.call-update) | async-done | bytes 2097168 | tf_op jit(solution)/shard_map/all_gather | solution.py:98
  288.0 3.1 constant_dynamic-update-slice_fusion
  291.1 8.0 %fusion.29 = bf16[256,3072]{1,0:T(8,128)(2,1)S(1)} fusion(bf16[2048,3072]{1,0:T(8,128)(2,1)} %constant_dynamic-update-slice_fusion, f32[256]{0:T(256)S(1)} %add_rsqrt_fusion.1, bf16[256,2048]{1,0:T(8,128)(2,1)S(1)} %copy-done.3, f32[2048]{0:T(1024)S(1)} %copy-done.10), kind=kOutput, calls=%fused_computation.44 | convolution fusion | flops 3224371200 | bytes 15213568 | tf_op jit(solution)/shard_map/dot_general | solution.py:106
  301.9 48.2 %while.30 = (s32[]{:T(128)}, f32[4,128,128]{2,1,0:T(8,128)S(1)}, f32[4,128]{1,0:T(4,128)S(1)}, f32[4,4,64,128]{3,2,0,1:T(8,128)}, f32[4,4,64,128]{3,2,0,1:T(8,12...) while((s32[]{:T(128)}, f32[4,128,128]{2,1,0:T(8,128)S(1)}, ...), condition=%wide.region_3.4_spmd.clone, body=%wide.region_1.3_spmd.clone.sunk | while | flops 140923904 | bytes 20806288 | solution.py:68
  302.3 1.7 exponential_select_fusion.2
  304.0 7.3 %fusion.136 = f32[4,64,64]{1,2,0:T(8,128)S(1)} fusion(f32[4,64,64,128]{3,2,1,0:T(8,128)S(1)} %exponential_select_fusion.2, f32[4,128,64]{1,2,0:T(8,128)S(1)} %dynamic-slice_bitcast_fusion.9, f32[4,128,64]{1,2,0:T(8,128)S(1)} %get-tuple-element.298), kind=kLoop, calls=%fused_computation.4.clone.1 | loop fusion | flops 6275072 | bytes 8716288 | tf_op jit(solution)/shard_map/while/body/eval_jaxpr/htk,hsk,htsk->hts/dot_general | solution.py:52
  314.3 1.7 exponential_select_fusion.2
  316.0 7.3 %fusion.136 = f32[4,64,64]{1,2,0:T(8,128)S(1)} fusion(f32[4,64,64,128]{3,2,1,0:T(8,128)S(1)} %exponential_select_fusion.2, f32[4,128,64]{1,2,0:T(8,128)S(1)} %dynamic-slice_bitcast_fusion.9, f32[4,128,64]{1,2,0:T(8,128)S(1)} %get-tuple-element.298), kind=kLoop, calls=%fused_computation.4.clone.1 | loop fusion | flops 6275072 | bytes 8716288 | tf_op jit(solution)/shard_map/while/body/eval_jaxpr/htk,hsk,htsk->hts/dot_general | solution.py:52
  326.3 1.7 exponential_select_fusion.2
  328.0 7.3 %fusion.136 = f32[4,64,64]{1,2,0:T(8,128)S(1)} fusion(f32[4,64,64,128]{3,2,1,0:T(8,128)S(1)} %exponential_select_fusion.2, f32[4,128,64]{1,2,0:T(8,128)S(1)} %dynamic-slice_bitcast_fusion.9, f32[4,128,64]{1,2,0:T(8,128)S(1)} %get-tuple-element.298), kind=kLoop, calls=%fused_computation.4.clone.1 | loop fusion | flops 6275072 | bytes 8716288 | tf_op jit(solution)/shard_map/while/body/eval_jaxpr/htk,hsk,htsk->hts/dot_general | solution.py:52
  338.3 1.7 exponential_select_fusion.2
  340.0 7.3 %fusion.136 = f32[4,64,64]{1,2,0:T(8,128)S(1)} fusion(f32[4,64,64,128]{3,2,1,0:T(8,128)S(1)} %exponential_select_fusion.2, f32[4,128,64]{1,2,0:T(8,128)S(1)} %dynamic-slice_bitcast_fusion.9, f32[4,128,64]{1,2,0:T(8,128)S(1)} %get-tuple-element.298), kind=kLoop, calls=%fused_computation.4.clone.1 | loop fusion | flops 6275072 | bytes 8716288 | tf_op jit(solution)/shard_map/while/body/eval_jaxpr/htk,hsk,htsk->hts/dot_general | solution.py:52
  353.2 2.1 collective-permute-start
  355.4 19.7 %all-gather.2 = f32[16,4,128]{2,1,0:T(4,128)S(1)} all-gather(f32[1,4,128]{2,1,0:T(4,128)S(1)} %exponential_bitcast_fusion), channel_id=2, replica_groups=mesh['sp'=16,'tp'=2] {'sp'}, dimensions={0}, use_global_device_ids=true | all-gather | bytes 34816 | tf_op jit(solution)/shard_map/all_gather | solution.py:14
  375.1 1.7 fusion.103
  377.0 23.2 %all-gather.32.cloned.1.call-done = f32[64,128,128]{2,1,0:T(8,128)} async-done(((f32[4,128,128]{2,1,0:T(8,128)}), f32[64,128,128]{2,1,0:T(8,128)}) %all-gather.32.cloned.1.call-update) | async-done | bytes 4194320 | tf_op jit(solution)/shard_map/all_gather | solution.py:14
  403.2 38.8 %all-gather.28.cloned.1.call-done = bf16[512,2048]{1,0:T(8,128)(2,1)} async-done(((bf16[512,128]{1,0:T(8,128)(2,1)}), bf16[512,2048]{1,0:T(8,128)(2,1)}) %all-gather.28.cloned.1.call-update) | async-done | bytes 2097168 | tf_op jit(solution)/shard_map/all_gather | solution.py:173
  442.0 42.2 %all-gather.30.cloned.1.call-done = bf16[512,2048]{1,0:T(8,128)(2,1)} async-done(((bf16[512,128]{1,0:T(8,128)(2,1)}), bf16[512,2048]{1,0:T(8,128)(2,1)}) %all-gather.30.cloned.1.call-update) | async-done | bytes 2097168 | tf_op jit(solution)/shard_map/all_gather | solution.py:174
  484.1 4.5 fusion.30
  488.6 19.6 %reduce-scatter.2.cloned.1.call-done = bf16[128,2048]{1,0:T(8,128)(2,1)} async-done(((bf16[256,2048]{1,0:T(8,128)(2,1)}), bf16[128,2048]{1,0:T(8,128)(2,1)}) %reduce-scatter.2.cloned.1.call-update) | async-done | bytes 524304 | tf_op jit(solution)/shard_map/reduce_scatter | solution.py:178
  509.5 2.0 fusion.39
  (126 shorter events, 29.7 us)
Async XLA Ops:
  6.5 368.5 %copy-start = (bf16[4,128,128]{2,1,0:T(8,128)(2,1)S(1)}, bf16[4,128,128]{2,1,0:T(8,128)(2,1)}, u32[]{:S(2)}) copy-start(bf16[4,128,128]{2,1,0:T(8,128)(2,1)} %param.31) | copy-start | bytes 393220
  6.5 26.4 %all-gather.14.cloned.1.call-start = ((), (), s32[]{:S(2)}) async-start(), calls=%async_computation.1 | async-start | bytes 1572864 | tf_op jit(solution)/shard_map/all_gather | solution.py:104
  7.3 69.3 %all-gather.16.cloned.1.call-start = ((), (), s32[]{:S(2)}) async-start(), calls=%async_computation.2 | async-start | bytes 2228224 | tf_op jit(solution)/shard_map/all_gather | solution.py:93
  8.0 110.9 %all-gather.18.cloned.1.call-start = ((), (), s32[]{:S(2)}) async-start(), calls=%async_computation.3 | async-start | bytes 2228224 | tf_op jit(solution)/shard_map/all_gather | solution.py:94
  8.7 152.4 %all-gather.20.cloned.1.call-start = ((), (), s32[]{:S(2)}) async-start(), calls=%async_computation.4 | async-start | bytes 2228224 | tf_op jit(solution)/shard_map/all_gather | solution.py:95
  9.3 194.1 %all-gather.22.cloned.1.call-start = ((), (), s32[]{:S(2)}) async-start(), calls=%async_computation.5 | async-start | bytes 2228224 | tf_op jit(solution)/shard_map/all_gather | solution.py:96
  9.9 235.7 %all-gather.24.cloned.1.call-start = ((), (), s32[]{:S(2)}) async-start(), calls=%async_computation.6 | async-start | bytes 2228224 | tf_op jit(solution)/shard_map/all_gather | solution.py:97
  10.5 277.5 %all-gather.26.cloned.1.call-start = ((), (), s32[]{:S(2)}) async-start(), calls=%async_computation.7 | async-start | bytes 2228224 | tf_op jit(solution)/shard_map/all_gather | solution.py:98
  11.2 389.0 %all-gather.32.cloned.1.call-start = ((), (), s32[]{:S(2)}) async-start(), calls=%async_computation.11 | async-start | bytes 4456448 | tf_op jit(solution)/shard_map/all_gather | solution.py:14
  206.6 84.5 %copy-start.3 = (bf16[256,2048]{1,0:T(8,128)(2,1)S(1)}, bf16[256,2048]{1,0:T(8,128)(2,1)}, u32[]{:S(2)}) copy-start(bf16[256,2048]{1,0:T(8,128)(2,1)} %all-gather.14.cloned.1.call-done) | copy-start | bytes 3145732
  206.6 84.5 %copy-start.10 = (f32[2048]{0:T(1024)S(1)}, f32[2048]{0:T(1024)}, u32[]{:S(2)}) copy-start(f32[2048]{0:T(1024)} %param.21) | copy-start | bytes 24580
  299.1 1.7 copy-start.2
  301.9 73.2 %copy-start.4 = (f32[256,512]{1,0:T(8,128)S(1)}, f32[256,512]{1,0:T(8,128)}, u32[]{:S(2)}) copy-start(f32[256,512]{1,0:T(8,128)} %get-tuple-element.180) | copy-start | bytes 1572868
  350.1 0.7 copy-start.1
  350.9 91.1 %all-gather.28.cloned.1.call-start = ((), (), s32[]{:S(2)}) async-start(), calls=%async_computation.8 | async-start | bytes 2228224 | tf_op jit(solution)/shard_map/all_gather | solution.py:173
  351.6 132.5 %all-gather.30.cloned.1.call-start = ((), (), s32[]{:S(2)}) async-start(), calls=%async_computation.9 | async-start | bytes 2228224 | tf_op jit(solution)/shard_map/all_gather | solution.py:174
  352.2 156.1 %reduce-scatter.2.cloned.1.call-start = ((), (), s32[]{:S(2)}) async-start(), calls=%async_computation.10 | async-start | bytes 1572864 | tf_op jit(solution)/shard_map/reduce_scatter | solution.py:178
  353.2 21.8 %collective-permute-start = (bf16[16,512]{1,0:T(8,128)(2,1)S(1)}, bf16[16,512]{1,0:T(8,128)(2,1)S(1)}, u32[]{:S(2)}, u32[]{:S(2)}) collective-permute-start(bf16[16,512]{1,0:T(8,128)(2,1)S(1)} %slice.99), channel_id=1, source_target_pairs={{0,2},{2,4},{4,6},{6,8},{8,10},{10,12},{12,14},{14,16},{16,18},{18... | collective-permute-start | bytes 49160 | tf_op jit(solution)/shard_map/ppermute | solution.py:28
  376.8 23.4 %copy-start.5 = (f32[4,4,64,128]{3,2,0,1:T(8,128)S(1)}, f32[4,4,64,128]{3,2,0,1:T(8,128)}, u32[]{:S(2)}) copy-start(f32[4,4,64,128]{3,2,0,1:T(8,128)} %get-tuple-element.104) | copy-start | bytes 1572868
  376.8 23.4 %copy-start.6 = (f32[4,4,64,128]{3,2,0,1:T(8,128)S(1)}, f32[4,4,64,128]{3,2,0,1:T(8,128)}, u32[]{:S(2)}) copy-start(f32[4,4,64,128]{3,2,0,1:T(8,128)} %get-tuple-element.108) | copy-start | bytes 1572868
  377.0 24.8 %copy-start.8 = (f32[512]{0:T(512)S(1)}, f32[512]{0:T(512)}, u32[]{:S(2)}) copy-start(f32[512]{0:T(512)} %param.30) | copy-start | bytes 6148
  377.0 24.8 %copy-start.9 = (f32[512]{0:T(512)S(1)}, f32[512]{0:T(512)}, u32[]{:S(2)}) copy-start(f32[512]{0:T(512)} %param.32) | copy-start | bytes 6148
  484.1 25.4 %copy-start.7 = (f32[2048]{0:T(1024)S(1)}, f32[2048]{0:T(1024)}, u32[]{:S(2)}) copy-start(f32[2048]{0:T(1024)} %param.35) | copy-start | bytes 24580
Sparse Core Ops, SparseCore 0:
  8.9 23.9 all-gather.13
  35.1 41.4 all-gather.15
  78.7 40.1 all-gather.17
  121.0 40.1 all-gather.19
  163.2 40.1 all-gather.21
  205.4 40.1 all-gather.23
  247.8 40.1 all-gather.25
  351.0 49.1 all-gather.31
  402.4 39.5 all-gather.27
  444.0 40.1 all-gather.29
  488.8 19.4 reduce-scatter.1
where the time goes:
time: 519 us; the launch traced here: 518 us
  waiting for transfers between devices  387 us (75%)
  other arithmetic  47.9 us (9%)
  local copies, waits for them, and re-layouts  23.9 us (5%)
  matrix products  23.2 us (4%)
  blocking collectives  19.7 us (4%)
  between operations  13.6 us (3%)
    all_gather x1, waiting for transfers between devices, per_device(): lax.all_gather(out_pool, 'sp', axis=1, tiled=True)  42.2 us
    all_gather x1, waiting for transfers between devices, per_device(): lax.all_gather(w_query, 'sp', axis=0, tiled=True)  42.1 us
    all_gather x1, waiting for transfers between devices, per_device(): lax.all_gather(w_forget, 'sp', axis=0, tiled=True)  39.2 us
    all_gather x1, waiting for transfers between devices, per_device(): lax.all_gather(w_pgate, 'sp', axis=0, tiled=True)  39.1 us
    all_gather x1, waiting for transfers between devices, per_device(): lax.all_gather(w_rgate, 'sp', axis=0, tiled=True)  39.1 us
    all_gather x1, waiting for transfers between devices, per_device(): lax.all_gather(w_pool_in, 'sp', axis=0, tiled=True)  39 us
    all_gather x1, waiting for transfers between devices, per_device(): lax.all_gather(w_input, 'sp', axis=0, tiled=True)  39 us
    all_gather x1, waiting for transfers between devices, per_device(): lax.all_gather(out_rec, 'sp', axis=1, tiled=True)  38.8 us
  transfers between devices with their start and end apart: 12, of which 11 were waited for; matrix products, arithmetic and copies ran while one was open for 5% of the time, Pallas kernels for 0%

commit v1 on v0

--- a/solution.py
+++ b/solution.py
@@ -89,9 +89,18 @@
     out_pool,
     post_gain,
 ):
+    switch_view_for = lambda original: jnp.concatenate(
+        jax.lax.all_to_all(
+            jnp.stack([original for _ in range(jax.lax.psum(1, axis_name="sp"))]),
+            axis_name="sp",
+            split_axis=0,
+            concat_axis=0,
+        ),
+        axis=0,
+    )
     gathered = (
         lax.all_gather(w_query, "sp", axis=0, tiled=True),
-        lax.all_gather(w_forget, "sp", axis=0, tiled=True),
+        switch_view_for(w_forget),
         lax.all_gather(w_input, "sp", axis=0, tiled=True),
         lax.all_gather(w_rgate, "sp", axis=0, tiled=True),
         lax.all_gather(w_pool_in, "sp", axis=0, tiled=True),

time: 519 us -> 487 us (0.938)
  waiting for transfers between devices: 387 us -> 348 us
  starting transfers between devices: 2.51 us -> 9.89 us
    all_gather x1 -> x0, waiting for transfers between devices: 39.2 us -> none  [per_device(): lax.all_gather(w_forget, 'sp', axis=0, tiled=True)]
    all_gather x1, waiting for transfers between devices: 42.1 us -> 51.7 us  [per_device(): lax.all_gather(w_query, 'sp', axis=0, tiled=True)]
    all_gather x1, waiting for transfers between devices: 20.1 us -> 12.2 us  [per_device(): lax.all_gather(tokens_in, 'tp', axis=1, tiled=True).astype(jnp.float32)]
    all_to_all x0 -> x1, starting transfers between devices: none -> 7.41 us  [per_device(): jax.lax.all_to_all(jnp.stack([original for _ in range(jax.lax.psum(1, axi...]
    unnamed x29 -> x33, local copies, waits for them, and re-layouts: 17.6 us -> 15.2 us
  transfers between devices with their start and end apart: 12 -> 12, of which waited for: 11 -> 10; matrix products, arithmetic and copies ran while one was open for 5% -> 5% of each run, Pallas kernels for 0% -> 0%
where the time goes in v1:
time: 487 us; the launch traced here: 486 us
  waiting for transfers between devices  348 us (71%)
  other arithmetic  47.3 us (10%)
  local copies, waits for them, and re-layouts  24.1 us (5%)
  matrix products  23.2 us (5%)
  blocking collectives  19.8 us (4%)
  between operations  13.9 us (3%)
  starting transfers between devices  9.89 us (2%)
    all_gather x1, waiting for transfers between devices, per_device(): lax.all_gather(w_query, 'sp', axis=0, tiled=True)  51.7 us
    all_gather x1, waiting for transfers between devices, per_device(): lax.all_gather(out_pool, 'sp', axis=1, tiled=True)  42.3 us
    all_gather x1, waiting for transfers between devices, per_device(): lax.all_gather(w_pool_in, 'sp', axis=0, tiled=True)  39.1 us
    all_gather x1, waiting for transfers between devices, per_device(): lax.all_gather(w_pgate, 'sp', axis=0, tiled=True)  39.1 us
    all_gather x1, waiting for transfers between devices, per_device(): lax.all_gather(w_rgate, 'sp', axis=0, tiled=True)  39 us
    all_gather x1, waiting for transfers between devices, per_device(): lax.all_gather(out_rec, 'sp', axis=1, tiled=True)  38.7 us
    all_gather x1, waiting for transfers between devices, per_device(): lax.all_gather(w_input, 'sp', axis=0, tiled=True)  38 us
    dot_general x4, other arithmetic, advance(): jnp.einsum('htk,hsk,htsk->hts', probe_segment, key_piece, weight, precisi...  29.3 us
  transfers between devices with their start and end apart: 12, of which 10 were waited for; matrix products, arithmetic and copies ran while one was open for 5% of the time, Pallas kernels for 0%

profile of v1, /device:TPU:0, one launch (start us, length us, event | category | flops | bytes accessed | tf_op | source)
XLA Modules:
  0.0 486.3 jit_solution(6207463690552763551)
XLA Ops:
  9.9 2.5 stack.2
  12.4 7.4 %all-to-all-start = ((bf16[16,128,512]{2,1,0:T(8,128)(2,1)}), bf16[16,128,512]{2,1,0:T(8,128)(2,1)S(1)}, u32[]{:S(2)}, u32[]{:S(2)}) async-start(bf16[16,128,512]{2,1,0:T(8,128)(2,1)} %stack.2), calls=%async_computation | async-start | bytes 4194304 | tf_op jit(solution)/shard_map/all_to_all | solution.py:93
  20.7 12.2 %all-gather.13.cloned.1.call-done = bf16[256,2048]{1,0:T(8,128)(2,1)} async-done(((bf16[256,1024]{1,0:T(8,128)(2,1)}), bf16[256,2048]{1,0:T(8,128)(2,1)}) %all-gather.13.cloned.1.call-update) | async-done | bytes 1048592 | tf_op jit(solution)/shard_map/all_gather | solution.py:113
  34.4 51.7 %all-gather.15.cloned.1.call-done = bf16[2048,512]{1,0:T(8,128)(2,1)} async-done(((bf16[128,512]{1,0:T(8,128)(2,1)}), bf16[2048,512]{1,0:T(8,128)(2,1)}) %all-gather.15.cloned.1.call-update) | async-done | bytes 2097168 | tf_op jit(solution)/shard_map/all_gather | solution.py:102
  86.2 3.1 constant_dynamic-update-slice_fusion.5
  90.9 38.0 %all-gather.17.cloned.1.call-done = bf16[2048,512]{1,0:T(8,128)(2,1)} async-done(((bf16[128,512]{1,0:T(8,128)(2,1)}), bf16[2048,512]{1,0:T(8,128)(2,1)}) %all-gather.17.cloned.1.call-update) | async-done | bytes 2097168 | tf_op jit(solution)/shard_map/all_gather | solution.py:104
  128.9 3.2 constant_dynamic-update-slice_fusion.3
  132.1 39.0 %all-gather.19.cloned.1.call-done = bf16[2048,512]{1,0:T(8,128)(2,1)} async-done(((bf16[128,512]{1,0:T(8,128)(2,1)}), bf16[2048,512]{1,0:T(8,128)(2,1)}) %all-gather.19.cloned.1.call-update) | async-done | bytes 2097168 | tf_op jit(solution)/shard_map/all_gather | solution.py:105
  171.1 3.1 constant_dynamic-update-slice_fusion.2
  174.3 39.1 %all-gather.21.cloned.1.call-done = bf16[2048,512]{1,0:T(8,128)(2,1)} async-done(((bf16[128,512]{1,0:T(8,128)(2,1)}), bf16[2048,512]{1,0:T(8,128)(2,1)}) %all-gather.21.cloned.1.call-update) | async-done | bytes 2097168 | tf_op jit(solution)/shard_map/all_gather | solution.py:106
  213.4 3.2 constant_dynamic-update-slice_fusion.1
  216.5 39.1 %all-gather.23.cloned.1.call-done = bf16[2048,512]{1,0:T(8,128)(2,1)} async-done(((bf16[128,512]{1,0:T(8,128)(2,1)}), bf16[2048,512]{1,0:T(8,128)(2,1)}) %all-gather.23.cloned.1.call-update) | async-done | bytes 2097168 | tf_op jit(solution)/shard_map/all_gather | solution.py:107
  255.6 3.2 constant_dynamic-update-slice_fusion
  258.8 8.0 %fusion.29 = bf16[256,3072]{1,0:T(8,128)(2,1)S(1)} fusion(bf16[2048,3072]{1,0:T(8,128)(2,1)} %constant_dynamic-update-slice_fusion, f32[256]{0:T(256)S(1)} %add_rsqrt_fusion.1, bf16[256,2048]{1,0:T(8,128)(2,1)S(1)} %copy-done.3, f32[2048]{0:T(1024)S(1)} %copy-done.12), kind=kOutput, calls=%fused_computation.44 | convolution fusion | flops 3224371200 | bytes 15213568 | tf_op jit(solution)/shard_map/dot_general | solution.py:115
  269.6 48.3 %while.30 = (s32[]{:T(128)}, f32[4,128,128]{2,1,0:T(8,128)S(1)}, f32[4,128]{1,0:T(4,128)S(1)}, f32[4,4,64,128]{3,2,0,1:T(8,128)}, f32[4,4,64,128]{3,2,0,1:T(8,12...) while((s32[]{:T(128)}, f32[4,128,128]{2,1,0:T(8,128)S(1)}, ...), condition=%wide.region_3.4_spmd.clone, body=%wide.region_1.3_spmd.clone.sunk | while | flops 140923904 | bytes 20806288 | solution.py:68
  270.0 1.7 exponential_select_fusion.2
  271.7 7.3 %fusion.136 = f32[4,64,64]{1,2,0:T(8,128)S(1)} fusion(f32[4,64,64,128]{3,2,1,0:T(8,128)S(1)} %exponential_select_fusion.2, f32[4,128,64]{1,2,0:T(8,128)S(1)} %dynamic-slice_bitcast_fusion.9, f32[4,128,64]{1,2,0:T(8,128)S(1)} %get-tuple-element.298), kind=kLoop, calls=%fused_computation.4.clone.1 | loop fusion | flops 6275072 | bytes 8716288 | tf_op jit(solution)/shard_map/while/body/eval_jaxpr/htk,hsk,htsk->hts/dot_general | solution.py:52
  282.0 1.7 exponential_select_fusion.2
  283.7 7.3 %fusion.136 = f32[4,64,64]{1,2,0:T(8,128)S(1)} fusion(f32[4,64,64,128]{3,2,1,0:T(8,128)S(1)} %exponential_select_fusion.2, f32[4,128,64]{1,2,0:T(8,128)S(1)} %dynamic-slice_bitcast_fusion.9, f32[4,128,64]{1,2,0:T(8,128)S(1)} %get-tuple-element.298), kind=kLoop, calls=%fused_computation.4.clone.1 | loop fusion | flops 6275072 | bytes 8716288 | tf_op jit(solution)/shard_map/while/body/eval_jaxpr/htk,hsk,htsk->hts/dot_general | solution.py:52
  294.0 1.7 exponential_select_fusion.2
  295.8 7.3 %fusion.136 = f32[4,64,64]{1,2,0:T(8,128)S(1)} fusion(f32[4,64,64,128]{3,2,1,0:T(8,128)S(1)} %exponential_select_fusion.2, f32[4,128,64]{1,2,0:T(8,128)S(1)} %dynamic-slice_bitcast_fusion.9, f32[4,128,64]{1,2,0:T(8,128)S(1)} %get-tuple-element.298), kind=kLoop, calls=%fused_computation.4.clone.1 | loop fusion | flops 6275072 | bytes 8716288 | tf_op jit(solution)/shard_map/while/body/eval_jaxpr/htk,hsk,htsk->hts/dot_general | solution.py:52
  306.1 1.7 exponential_select_fusion.2
  307.8 7.3 %fusion.136 = f32[4,64,64]{1,2,0:T(8,128)S(1)} fusion(f32[4,64,64,128]{3,2,1,0:T(8,128)S(1)} %exponential_select_fusion.2, f32[4,128,64]{1,2,0:T(8,128)S(1)} %dynamic-slice_bitcast_fusion.9, f32[4,128,64]{1,2,0:T(8,128)S(1)} %get-tuple-element.298), kind=kLoop, calls=%fused_computation.4.clone.1 | loop fusion | flops 6275072 | bytes 8716288 | tf_op jit(solution)/shard_map/while/body/eval_jaxpr/htk,hsk,htsk->hts/dot_general | solution.py:52
  321.2 2.1 collective-permute-start
  323.3 19.8 %all-gather.2 = f32[16,4,128]{2,1,0:T(4,128)S(1)} all-gather(f32[1,4,128]{2,1,0:T(4,128)S(1)} %exponential_bitcast_fusion), channel_id=2, replica_groups=mesh['sp'=16,'tp'=2] {'sp'}, dimensions={0}, use_global_device_ids=true | all-gather | bytes 34816 | tf_op jit(solution)/shard_map/all_gather | solution.py:14
  343.1 1.7 fusion.103
  345.1 22.9 %all-gather.29.cloned.1.call-done = f32[64,128,128]{2,1,0:T(8,128)} async-done(((f32[4,128,128]{2,1,0:T(8,128)}), f32[64,128,128]{2,1,0:T(8,128)}) %all-gather.29.cloned.1.call-update) | async-done | bytes 4194320 | tf_op jit(solution)/shard_map/all_gather | solution.py:14
  371.0 38.7 %all-gather.25.cloned.1.call-done = bf16[512,2048]{1,0:T(8,128)(2,1)} async-done(((bf16[512,128]{1,0:T(8,128)(2,1)}), bf16[512,2048]{1,0:T(8,128)(2,1)}) %all-gather.25.cloned.1.call-update) | async-done | bytes 2097168 | tf_op jit(solution)/shard_map/all_gather | solution.py:182
  409.7 42.3 %all-gather.27.cloned.1.call-done = bf16[512,2048]{1,0:T(8,128)(2,1)} async-done(((bf16[512,128]{1,0:T(8,128)(2,1)}), bf16[512,2048]{1,0:T(8,128)(2,1)}) %all-gather.27.cloned.1.call-update) | async-done | bytes 2097168 | tf_op jit(solution)/shard_map/all_gather | solution.py:183
  452.1 4.5 fusion.30
  456.6 19.6 %reduce-scatter.2.cloned.1.call-done = bf16[128,2048]{1,0:T(8,128)(2,1)} async-done(((bf16[256,2048]{1,0:T(8,128)(2,1)}), bf16[128,2048]{1,0:T(8,128)(2,1)}) %reduce-scatter.2.cloned.1.call-update) | async-done | bytes 524304 | tf_op jit(solution)/shard_map/reduce_scatter | solution.py:187
  477.5 2.0 fusion.39
  (130 shorter events, 29.4 us)
Async XLA Ops:
  6.5 336.6 %copy-start = (bf16[4,128,128]{2,1,0:T(8,128)(2,1)S(1)}, bf16[4,128,128]{2,1,0:T(8,128)(2,1)}, u32[]{:S(2)}) copy-start(bf16[4,128,128]{2,1,0:T(8,128)(2,1)} %param.31) | copy-start | bytes 393220
  6.5 14.0 %copy-start.8 = (f32[256,4]{0,1:T(4,128)S(1)}, f32[256,4]{0,1:T(4,128)}, u32[]{:S(2)}) copy-start(f32[256,4]{0,1:T(4,128)} %param.29) | copy-start | bytes 12292
  6.5 14.1 %copy-start.11 = (f32[512]{0:T(512)S(1)}, f32[512]{0:T(512)}, u32[]{:S(2)}) copy-start(f32[512]{0:T(512)} %param.28) | copy-start | bytes 6148
  6.5 26.4 %all-gather.13.cloned.1.call-start = ((), (), s32[]{:S(2)}) async-start(), calls=%async_computation.2 | async-start | bytes 1572864 | tf_op jit(solution)/shard_map/all_gather | solution.py:113
  7.3 78.9 %all-gather.15.cloned.1.call-start = ((), (), s32[]{:S(2)}) async-start(), calls=%async_computation.3 | async-start | bytes 2228224 | tf_op jit(solution)/shard_map/all_gather | solution.py:102
  8.0 120.9 %all-gather.17.cloned.1.call-start = ((), (), s32[]{:S(2)}) async-start(), calls=%async_computation.4 | async-start | bytes 2228224 | tf_op jit(solution)/shard_map/all_gather | solution.py:104
  8.7 162.4 %all-gather.19.cloned.1.call-start = ((), (), s32[]{:S(2)}) async-start(), calls=%async_computation.5 | async-start | bytes 2228224 | tf_op jit(solution)/shard_map/all_gather | solution.py:105
  9.3 204.0 %all-gather.21.cloned.1.call-start = ((), (), s32[]{:S(2)}) async-start(), calls=%async_computation.6 | async-start | bytes 2228224 | tf_op jit(solution)/shard_map/all_gather | solution.py:106
  12.4 76.9 %all-to-all-start = ((bf16[16,128,512]{2,1,0:T(8,128)(2,1)}), bf16[16,128,512]{2,1,0:T(8,128)(2,1)S(1)}, u32[]{:S(2)}, u32[]{:S(2)}) async-start(bf16[16,128,512]{2,1,0:T(8,128)(2,1)} %stack.2), calls=%async_computation | async-start | bytes 4194304 | tf_op jit(solution)/shard_map/all_to_all | solution.py:93
  19.8 235.7 %all-gather.23.cloned.1.call-start = ((), (), s32[]{:S(2)}) async-start(), calls=%async_computation.7 | async-start | bytes 2228224 | tf_op jit(solution)/shard_map/all_gather | solution.py:107
  20.4 347.6 %all-gather.29.cloned.1.call-start = ((), (), s32[]{:S(2)}) async-start(), calls=%async_computation.11 | async-start | bytes 4456448 | tf_op jit(solution)/shard_map/all_gather | solution.py:14
  174.3 84.5 %copy-start.3 = (bf16[256,2048]{1,0:T(8,128)(2,1)S(1)}, bf16[256,2048]{1,0:T(8,128)(2,1)}, u32[]{:S(2)}) copy-start(bf16[256,2048]{1,0:T(8,128)(2,1)} %all-gather.13.cloned.1.call-done) | copy-start | bytes 3145732
  174.3 84.5 %copy-start.12 = (f32[2048]{0:T(1024)S(1)}, f32[2048]{0:T(1024)}, u32[]{:S(2)}) copy-start(f32[2048]{0:T(1024)} %param.21) | copy-start | bytes 24580
  266.8 1.7 copy-start.2
  269.6 73.5 %copy-start.4 = (f32[256,512]{1,0:T(8,128)S(1)}, f32[256,512]{1,0:T(8,128)}, u32[]{:S(2)}) copy-start(f32[256,512]{1,0:T(8,128)} %get-tuple-element.180) | copy-start | bytes 1572868
  317.9 0.7 copy-start.1
  318.7 91.1 %all-gather.25.cloned.1.call-start = ((), (), s32[]{:S(2)}) async-start(), calls=%async_computation.8 | async-start | bytes 2228224 | tf_op jit(solution)/shard_map/all_gather | solution.py:182
  319.4 132.6 %all-gather.27.cloned.1.call-start = ((), (), s32[]{:S(2)}) async-start(), calls=%async_computation.9 | async-start | bytes 2228224 | tf_op jit(solution)/shard_map/all_gather | solution.py:183
  320.1 156.1 %reduce-scatter.2.cloned.1.call-start = ((), (), s32[]{:S(2)}) async-start(), calls=%async_computation.10 | async-start | bytes 1572864 | tf_op jit(solution)/shard_map/reduce_scatter | solution.py:187
  321.2 21.9 %collective-permute-start = (bf16[16,512]{1,0:T(8,128)(2,1)S(1)}, bf16[16,512]{1,0:T(8,128)(2,1)S(1)}, u32[]{:S(2)}, u32[]{:S(2)}) collective-permute-start(bf16[16,512]{1,0:T(8,128)(2,1)S(1)} %slice.99), channel_id=1, source_target_pairs={{0,2},{2,4},{4,6},{6,8},{8,10},{10,12},{12,14},{14,16},{16,18},{18... | collective-permute-start | bytes 49160 | tf_op jit(solution)/shard_map/ppermute | solution.py:28
  344.8 23.2 %copy-start.5 = (f32[4,4,64,128]{3,2,0,1:T(8,128)S(1)}, f32[4,4,64,128]{3,2,0,1:T(8,128)}, u32[]{:S(2)}) copy-start(f32[4,4,64,128]{3,2,0,1:T(8,128)} %get-tuple-element.104) | copy-start | bytes 1572868
  344.8 23.2 %copy-start.6 = (f32[4,4,64,128]{3,2,0,1:T(8,128)S(1)}, f32[4,4,64,128]{3,2,0,1:T(8,128)}, u32[]{:S(2)}) copy-start(f32[4,4,64,128]{3,2,0,1:T(8,128)} %get-tuple-element.108) | copy-start | bytes 1572868
  345.0 24.6 %copy-start.9 = (f32[512]{0:T(512)S(1)}, f32[512]{0:T(512)}, u32[]{:S(2)}) copy-start(f32[512]{0:T(512)} %param.30) | copy-start | bytes 6148
  345.0 24.6 %copy-start.10 = (f32[512]{0:T(512)S(1)}, f32[512]{0:T(512)}, u32[]{:S(2)}) copy-start(f32[512]{0:T(512)} %param.32) | copy-start | bytes 6148
  452.0 25.4 %copy-start.7 = (f32[2048]{0:T(1024)S(1)}, f32[2048]{0:T(1024)}, u32[]{:S(2)}) copy-start(f32[2048]{0:T(1024)} %param.35) | copy-start | bytes 24580
Sparse Core Ops, SparseCore 0:
  8.9 23.9 all-gather.12
  35.1 51.0 all-gather.14
  88.3 40.5 all-gather.16
  130.9 40.1 all-gather.18
  173.1 40.1 all-gather.20
  215.4 40.1 all-gather.22
  318.8 49.1 all-gather.28
  370.1 39.5 all-gather.24
  411.9 40.1 all-gather.26
  456.7 19.4 reduce-scatter.1
